TPU v7x, 32 devices: a whole 2x2x4 slice. The times are simulated.
32 devices in a mesh: grp: 2 (over y), ep: 4 (over z), tp: 4 (over x, core).
Axes of the slice: x: 2, y: 2, z: 4, core: 2. Of those that a mesh axis runs over, the one named last changes fastest.
Arguments:
- tokens: bfloat16 [3072, 2048], P(('grp', 'ep'), 'tp'), parts along dimension 0
- group_choice: int32 [3072], P(('grp', 'ep')), parts along dimension 0, may hold values from 0 to 1, as said below
- expert_choice: int32 [3072, 2], P(('grp', 'ep')), parts along dimension 0, may hold values from 0 to 1, as said below
- group_weight: float32 [3072], P(('grp', 'ep')), parts along dimension 0, may hold values from 0.3 to 1
- expert_weight: float32 [3072, 2], P(('grp', 'ep')), parts along dimension 0, may hold values from 0.1 to 1
- norm_gain: float32 [2048], replicated, may hold values from 0.1 to 1.9
- w_gate: bfloat16 [4, 2048, 1024], P('ep', None, 'tp'), may hold values from -0.125 to 0.125
- w_up: bfloat16 [4, 2048, 1024], P('ep', None, 'tp'), may hold values from -0.125 to 0.125
- w_down: bfloat16 [4, 1024, 2048], P('ep', None, 'tp'), may hold values from -0.1875 to 0.1875
Outputs:
- moe_out: bfloat16 [3072, 2048], P(('grp', 'ep'), 'tp'), parts along dimension 0
There are 2 independent parts, one for each index of `grp`. A program takes and returns all parts, laid end to end along the dimension named above; an argument that names none is the same for every part. Nothing has to cross between parts.
Inputs may be any that keep to these rules, and one draw needn't show every extreme that they name: `group_choice`: group of each token, 0 to 1; within each aligned block of 384 tokens (the tokens of one index of ep) every group is chosen by the same number of tokens. `expert_choice`: a token's two entries differ; within each aligned block of 384 tokens no expert (group with entry) is named by more than 192 tokens, and in every block one expert of each group, the same one in all blocks, is named by exactly 192 tokens.
All inputs are finite; a program needn't handle non-finite values.
Results may differ from a plain program's by a relative error of at most 0.0071.
Values may be sent and summed in bfloat16 or wider, within the bound.
A program may use at most 64 MiB of HBM per device.

v0:
```python
import functools

import jax
import jax.numpy as jnp
from jax import lax
from jax.experimental import pallas as pl
from jax.experimental.pallas import tpu as pltpu
from jax.sharding import PartitionSpec as P

MESH = pl.DeviceIdType.MESH


def finish_rows(gate_sum, up_sum, w_down):
    hidden = (jax.nn.silu(gate_sum) * up_sum).astype(jnp.bfloat16)
    whole_hidden = lax.all_gather(hidden, "tp", axis=3, tiled=True)
    summed = jnp.einsum("sxcf,xfd->sxcd", whole_hidden, w_down, preferred_element_type=jnp.float32)
    return summed.astype(jnp.bfloat16)


def body(
    tokens,
    group_choice,
    expert_choice,
    group_weight,
    expert_weight,
    norm_gain,
    w_gate,
    w_up,
    w_down,
):
    tok_rows = tokens.shape[0]
    ep_count = lax.axis_size("ep")
    exp_local = w_gate.shape[0]
    experts_all = ep_count * exp_local
    group_size = min(8, experts_all // 2)
    group_count = experts_all // group_size
    mean_load = 2 * tok_rows // experts_all
    capacity = mean_load + min(mean_load // 2, tok_rows // group_count - mean_load)
    model_width = norm_gain.shape[0]
    expert_ids = group_choice[:, None] * group_size + expert_choice
    mixing = group_weight[:, None] * expert_weight / jnp.sum(expert_weight, -1, keepdims=True)
    flat_ids = expert_ids.reshape(-1)
    marks = (flat_ids[:, None] == jnp.arange(experts_all, dtype=jnp.int32)[None, :]).astype(
        jnp.int32
    )
    earlier = jnp.cumsum(marks, 0) - marks
    seat_index = jnp.sum(earlier * marks, 1)
    targets = (flat_ids * capacity + seat_index).reshape(tok_rows, 2)
    places = jnp.arange(experts_all * capacity, dtype=jnp.int32)
    dispatch = (
        (places[:, None] == targets[None, :, 0]) | (places[:, None] == targets[None, :, 1])
    ).astype(jnp.bfloat16)
    values = tokens.astype(jnp.float32)
    own_squares = jnp.sum(values * values, -1)
    all_squares = lax.psum(own_squares, "tp")
    inv_rms = lax.rsqrt(all_squares / model_width + 1e-06)
    piece_width = tokens.shape[1]
    gain_piece = lax.dynamic_slice_in_dim(
        norm_gain, lax.axis_index("tp") * piece_width, piece_width, 0
    )
    normed = (values * inv_rms[:, None] * gain_piece[None, :]).astype(jnp.bfloat16)
    buffer = jnp.dot(dispatch, normed, preferred_element_type=jnp.float32).astype(jnp.bfloat16)
    buffer = buffer.reshape(ep_count, exp_local, capacity, piece_width)
    piece = lax.all_gather(
        lax.all_to_all(buffer, "ep", split_axis=0, concat_axis=0, tiled=True),
        "tp",
        axis=3,
        tiled=True,
    )
    gate_next = jnp.einsum("sxcd,xdf->sxcf", piece, w_gate, preferred_element_type=jnp.float32)
    up_next = jnp.einsum("sxcd,xdf->sxcf", piece, w_up, preferred_element_type=jnp.float32)
    results = finish_rows(gate_next, up_next, w_down)
    returned = lax.all_to_all(results, "ep", split_axis=0, concat_axis=0, tiled=True)
    returned = returned.reshape(experts_all * capacity, returned.shape[3])
    combined = jnp.zeros((tok_rows, returned.shape[1]), jnp.float32)
    for choice_index in range(2):
        picker = (targets[:, choice_index : choice_index + 1] == places[None, :]).astype(
            jnp.bfloat16
        )
        picked = jnp.dot(picker, returned, preferred_element_type=jnp.float32)
        combined = combined + mixing[:, choice_index : choice_index + 1] * picked
    return combined.astype(jnp.bfloat16)


def layer_kernel(
    chunks,
    group_ref,
    choice_ref,
    group_weight_ref,
    expert_weight_ref,
    gain_ref,
    tok_ref,
    gate_hbm,
    up_hbm,
    down_hbm,
    out_ref,
    w_gate,
    w_up,
    w_down,
    rows,
    other,
    hid,
    outs,
    back,
    home,
    place,
    comb,
    mix_rows,
    mix_far,
    norm,
    wsem,
    z_send,
    z_recv,
    fwd_send,
    x_send,
    x_recv,
    h_send,
    h_recv,
    r_send,
    r_recv,
    c_send,
    c_recv,
    m_send,
    m_recv,
):
    z = lax.axis_index("ep")
    t = lax.axis_index("tp")
    group = z // 2
    parity = z % 2
    inner = (parity + group) % 2
    is_inner = inner == 1
    is_outer = inner == 0
    partner = z + 1 - 2 * parity
    cross = 2 - group
    cross_outer = 3 * (1 - group)
    near = t + 1 - 2 * (t % 2)
    far = (t + 2) % 4
    diag = (near + 2) % 4
    size, width = rows.shape[2:]
    half = size * chunks
    count = 2 * half
    items = 4 * chunks
    model_width = 4 * width
    hidden_width = hid.shape[3]

    loads = [
        pltpu.make_async_copy(source, target, wsem.at[i])
        for i, (source, target) in enumerate(
            ((gate_hbm, w_gate), (up_hbm, w_up), (down_hbm, w_down))
        )
    ]
    for load in loads:
        load.start()

    barrier = pltpu.get_barrier_semaphore()

    def greet(**where):
        pl.semaphore_signal(barrier, inc=1, device_id=where, device_id_type=MESH)

    greet(tp=near)
    greet(tp=far)
    greet(ep=partner)
    greet(ep=cross)

    @pl.when(is_inner)
    def _():
        greet(ep=cross_outer)

    def remote(source, target, send, recv, **where):
        return pltpu.make_async_remote_copy(
            src_ref=source,
            dst_ref=target,
            send_sem=send,
            recv_sem=recv,
            device_id=where,
            device_id_type=MESH,
        )

    def arrived(ref, sem):
        remote(ref, ref, sem, sem, tp=near).wait_recv()

    line = lax.broadcasted_iota(jnp.int32, (count, count), 0)
    lane = lax.broadcasted_iota(jnp.int32, (count, count), 1)
    eye = line == lane

    def column(row):
        return jnp.sum(jnp.where(eye, row, 0.0), 1, keepdims=True)

    own_row = jnp.where(group_ref[...].reshape(1, -1) == group, 1.0, 0.0)
    own_rows = jnp.broadcast_to(own_row, (8, count)).astype(jnp.bfloat16)
    earlier = jnp.where(line < lane, 1.0, 0.0).astype(jnp.bfloat16)
    before = jnp.dot(own_rows, earlier, preferred_element_type=jnp.float32)[0:1, :]
    at = lax.broadcasted_iota(jnp.int32, (1, count), 1).astype(jnp.float32)
    seat_row = jnp.where(own_row > 0.5, before, half + at - before)
    seat_ints = seat_row.astype(jnp.int32)

    def sort_half(start, target):
        want = lax.broadcasted_iota(jnp.int32, (half, count), 0) + start
        order = jnp.where(seat_ints == want, 1.0, 0.0).astype(jnp.bfloat16)
        part = jnp.dot(order, tok_ref[...], preferred_element_type=jnp.float32)
        for c in range(chunks):
            target(c, part[c * size : (c + 1) * size].astype(jnp.bfloat16))

    def keep_own(c, value):
        rows[c, t] = value

    def keep_other(c, value):
        other[c] = value

    sort_half(0, keep_own)

    pl.semaphore_wait(barrier, 4 + inner)

    slot = 3 - inner

    def own_send(c):
        there = chunks + c
        return remote(rows.at[c, t], rows.at[there, t], z_send.at[c], z_recv.at[there], ep=partner)

    def other_send(c):
        there = slot * chunks + c
        return remote(
            other.at[c], rows.at[there, t], z_send.at[chunks + c], z_recv.at[there], ep=cross
        )

    mix_send = remote(mix_rows, mix_far.at[slot - 2], m_send, m_recv.at[slot - 2], ep=cross)

    def spread(buffer, k, send, recv, step):
        mine = buffer.at[k, t]
        if step == 0:
            remote(mine, mine, send.at[k, 1], recv.at[k, 1], tp=far).start()
            remote(mine, mine, send.at[k, 0], recv.at[k, 0], tp=near).start()
        elif step == 1:
            theirs = buffer.at[k, far]
            arrived(theirs, recv.at[k, 1])
            remote(theirs, theirs, send.at[k, 2], recv.at[k, 2], tp=near).start()
        elif step == 2:
            arrived(buffer.at[k, near], recv.at[k, 0])
            arrived(buffer.at[k, diag], recv.at[k, 2])
        else:
            remote(mine, mine, send.at[k, 1], recv.at[k, 1], tp=far).wait_send()
            remote(mine, mine, send.at[k, 0], recv.at[k, 0], tp=near).wait_send()
            theirs = buffer.at[k, far]
            remote(theirs, theirs, send.at[k, 2], recv.at[k, 2], tp=near).wait_send()

    def relay(k):
        sem = fwd_send.at[k - 2 * chunks]
        return remote(rows.at[k, t], rows.at[k, t], sem, z_recv.at[k], ep=partner)

    def stage_a(k):
        if chunks <= k < 2 * chunks:
            arrived(rows.at[k, t], z_recv.at[k])
        if k >= 2 * chunks:
            pl.when(is_outer)(lambda: arrived(rows.at[k, t], z_recv.at[k]))
        spread(rows, k, x_send, x_recv, 0)

    def stage_r(k):
        @pl.when(is_inner)
        def _():
            arrived(rows.at[k, t], z_recv.at[k])
            relay(k).start()

    def stage_b(k):
        spread(rows, k, x_send, x_recv, 1)

    def stage_c(k):
        spread(rows, k, x_send, x_recv, 2)
        squares = jnp.zeros((size, 1), jnp.float32)
        for j in range(4):
            values = rows[k, j].astype(jnp.float32)
            squares = squares + jnp.sum(values * values, 1, keepdims=True)
        inv_rms = lax.rsqrt(squares / model_width + 1e-06)
        for j in range(4):
            cols = slice(j * width, (j + 1) * width)
            values = rows[k, j].astype(jnp.float32)
            norm[:, cols] = (values * inv_rms * gain_ref[0:1, cols]).astype(jnp.bfloat16)
        if k == 0:
            loads[0].wait()
            loads[1].wait()
        gate = jnp.dot(norm[...], w_gate[...], preferred_element_type=jnp.float32)
        up = jnp.dot(norm[...], w_up[...], preferred_element_type=jnp.float32)
        hid[k, t] = (gate / (1.0 + jnp.exp(-gate)) * up).astype(jnp.bfloat16)
        if k >= chunks:
            spread(hid, k, h_send, h_recv, 0)

    def stage_d(k):
        spread(hid, k, h_send, h_recv, 1)

    def back_send(k):
        there = k - chunks if k < 2 * chunks else k
        return remote(outs.at[k], back.at[there], r_send.at[k], r_recv.at[there], ep=partner)

    def stage_e(k):
        spread(hid, k, h_send, h_recv, 2)
        if k == chunks:
            loads[2].wait()
        total = jnp.zeros((size, width), jnp.float32)
        for j in range(4):
            part = w_down[j * hidden_width : (j + 1) * hidden_width, :]
            total = total + jnp.dot(hid[k, j], part, preferred_element_type=jnp.float32)
        outs[k] = total.astype(jnp.bfloat16)
        if chunks <= k < 2 * chunks:
            back_send(k).start()
        if k >= 2 * chunks:
            pl.when(is_outer)(lambda: back_send(k).start())

    def joined(k, mixes, start):
        arrived(back.at[k], r_recv.at[k])
        start = start + (k % chunks) * size
        low = lax.broadcasted_iota(jnp.int32, (size, count), 0) + start
        pick = low == lax.broadcasted_iota(jnp.int32, (size, count), 1)
        even = jnp.sum(jnp.where(pick, mixes[0:1, :], 0.0), 1, keepdims=True)
        odd = jnp.sum(jnp.where(pick, mixes[1:2, :], 0.0), 1, keepdims=True)
        mine = jnp.where(parity == 0, even, odd)
        theirs = jnp.where(parity == 0, odd, even)
        summed = mine * outs[k].astype(jnp.float32) + theirs * back[k].astype(jnp.float32)
        return summed.astype(jnp.bfloat16)

    def comb_send(k):
        where = cross if k < 3 * chunks else cross_outer
        i, c = k - 2 * chunks, k % chunks
        return remote(comb.at[i], home.at[c], c_send.at[i], c_recv.at[c], ep=where)

    def stage_j(k):
        @pl.when(is_inner)
        def _():
            far_slot = k // chunks - 2
            if k % chunks == 0:
                arrived(mix_far.at[far_slot], m_recv.at[far_slot])
            comb[k - 2 * chunks] = joined(k, mix_far[far_slot], half)
            comb_send(k).start()

    stage_a(0)
    for c in range(chunks):
        own_send(c).start()
    sort_half(half, keep_other)
    for c in range(chunks):
        other_send(c).start()
    stage_a(1)
    first, second = expert_weight_ref[0:1, :], expert_weight_ref[1:2, :]
    first_even = choice_ref[0:1, :] == 0
    scale = group_weight_ref[...].reshape(1, -1)
    both = first + second
    even_row = scale * jnp.where(first_even, first, second) / both
    odd_row = scale * jnp.where(first_even, second, first) / both
    seat_int = column(seat_row).astype(jnp.int32)
    taken = seat_int == lane
    mix_rows[0:1, :] = jnp.sum(jnp.where(taken, column(even_row), 0.0), 0, keepdims=True)
    mix_rows[1:2, :] = jnp.sum(jnp.where(taken, column(odd_row), 0.0), 0, keepdims=True)
    mix_send.start()
    wide = lax.broadcasted_iota(jnp.int32, (count, size), 1)
    for c in range(2 * chunks):
        place[c] = jnp.where(seat_int == wide + c * size, 1.0, 0.0).astype(jnp.bfloat16)
    for i in range(items + 2):
        if i < items:
            stage_b(i)
        if i < 2 * chunks:
            stage_r(i + 2 * chunks)
        if i + 2 < items:
            stage_a(i + 2)
        if i == items - 1:
            for k in range(chunks - 1):
                spread(hid, k, h_send, h_recv, 0)
        if i - 2 >= chunks:
            stage_d(i - 2)
        if i < items:
            stage_c(i)
        if i == items - 1:
            spread(hid, chunks - 1, h_send, h_recv, 0)
        if i - 2 >= chunks:
            stage_e(i - 2)
        if i - 4 >= 2 * chunks:
            stage_j(i - 4)
    for k in range(chunks):
        stage_d(k)
    for n, k in enumerate(range(max(items - 2, 2 * chunks), items)):
        if n < chunks:
            stage_e(n)
        stage_j(k)
    for k in range(min(2, chunks), chunks):
        stage_e(k)
    result = jnp.zeros((count, width), jnp.float32)
    for c in range(chunks):
        done = joined(c, mix_rows[...], 0)
        result = result + jnp.dot(place[c], done, preferred_element_type=jnp.float32)
    for c in range(chunks):
        arrived(home.at[c], c_recv.at[c])
        done = home[c]
        result = result + jnp.dot(place[chunks + c], done, preferred_element_type=jnp.float32)
    out_ref[...] = result.astype(jnp.bfloat16)

    for c in range(chunks):
        own_send(c).wait_send()
        other_send(c).wait_send()
        back_send(chunks + c).wait_send()
    mix_send.wait_send()
    for k in range(items):
        spread(rows, k, x_send, x_recv, 3)
        spread(hid, k, h_send, h_recv, 3)

    @pl.when(is_inner)
    def _():
        for k in range(2 * chunks, items):
            relay(k).wait_send()
            comb_send(k).wait_send()

    @pl.when(is_outer)
    def _():
        for k in range(2 * chunks, items):
            back_send(k).wait_send()


CHUNKS = 2


def paired_body(
    tokens,
    group_choice,
    expert_choice,
    group_weight,
    expert_weight,
    norm_gain,
    w_gate,
    w_up,
    w_down,
):
    count, width = tokens.shape
    half = count // 2
    depth, hidden_width = w_gate.shape[1:]
    chunks = CHUNKS if half % (16 * CHUNKS) == 0 else 1
    size = half // chunks
    items = 4 * chunks
    bf16 = jnp.bfloat16
    dma = pltpu.SemaphoreType.DMA
    vmem = pl.BlockSpec(memory_space=pltpu.VMEM)
    anywhere = pl.BlockSpec(memory_space=pl.ANY)
    return pl.pallas_call(
        functools.partial(layer_kernel, chunks),
        out_shape=jax.ShapeDtypeStruct((count, width), bf16),
        in_specs=[vmem] * 6 + [anywhere] * 3,
        out_specs=vmem,
        scratch_shapes=[
            pltpu.VMEM((depth, hidden_width), bf16),
            pltpu.VMEM((depth, hidden_width), bf16),
            pltpu.VMEM(w_down.shape[1:], bf16),
            pltpu.VMEM((items, 4, size, width), bf16),
            pltpu.VMEM((chunks, size, width), bf16),
            pltpu.VMEM((items, 4, size, hidden_width), bf16),
            pltpu.VMEM((items, size, width), bf16),
            pltpu.VMEM((items, size, width), bf16),
            pltpu.VMEM((chunks, size, width), bf16),
            pltpu.VMEM((2 * chunks, count, size), bf16),
            pltpu.VMEM((2 * chunks, size, width), bf16),
            pltpu.VMEM((8, count), jnp.float32),
            pltpu.VMEM((2, 8, count), jnp.float32),
            pltpu.VMEM((size, depth), bf16),
            dma((3,)),
            dma((2 * chunks,)),
            dma((items,)),
            dma((2 * chunks,)),
            dma((items, 3)),
            dma((items, 3)),
            dma((items, 3)),
            dma((items, 3)),
            dma((items,)),
            dma((items,)),
            dma((2 * chunks,)),
            dma((chunks,)),
            dma,
            dma((2,)),
        ],
        compiler_params=pltpu.CompilerParams(
            collective_id=0, has_side_effects=True, vmem_limit_bytes=56 * 1024 * 1024
        ),
    )(
        group_choice,
        expert_choice.T,
        group_weight,
        expert_weight.T,
        norm_gain.reshape(1, -1),
        tokens,
        w_gate[0],
        w_up[0],
        w_down[0],
    )

def pick_body(mesh, *arrays):
    experts = arrays[6].shape[0]
    group_size = min(8, experts // 2)
    choices = arrays[2].shape[1]
    sizes = dict(mesh.shape)
    fits = group_size == choices and experts == 2 * group_size == sizes["ep"]
    return paired_body if fits and sizes["tp"] == sizes["ep"] else body


def solution(mesh):
    in_specs = (
        P(("grp", "ep"), "tp"),
        P(("grp", "ep")),
        P(("grp", "ep"), None),
        P(("grp", "ep")),
        P(("grp", "ep"), None),
        P(),
        P("ep", None, "tp"),
        P("ep", None, "tp"),
        P("ep", None, "tp"),
    )
    out_specs = P(("grp", "ep"), "tp")

    def layer(*arrays):
        run = jax.shard_map(
            pick_body(mesh, *arrays),
            mesh=mesh,
            in_specs=in_specs,
            out_specs=out_specs,
            check_vma=False,
        )
        return run(*arrays)

    return layer
```

profile of v0, /device:TPU:0, one launch (start us, length us, event | category | flops | bytes accessed | tf_op | source)
XLA Modules:
  0.0 49.7 jit_solution(5179636475896577447)
XLA Ops:
  0.0 47.9 %shard_map.91 = bf16[384,512]{1,0:T(8,128)(2,1)} custom-call(s32[384]{0:T(512)} %group_ref.1, s32[2,384]{1,0:T(2,128)} %bitcast.10, f32[384]{0:T(512)} %group_weight_ref.1, f32[2,384]{1,0:T(2,128)} %bitcast.11, f32[1,2048]{1,0:T(1,128)} %bitcast.9, bf16[384,512]{1,0:T(8,128)(2,1)} %tok_ref.1, bf16[2048,256]{1,0:T(8,128)(2,1)} %bitcast.6, ...), custom_call_target="tpu_custom_call" | custom-call | tf_op jit(solution)/shard_map/pallas_call | solution.py:437
  47.9 1.8 %copy.11 = bf16[384,512]{1,0:T(8,128)(2,1)} copy(bf16[384,512]{1,0:T(8,128)(2,1)} %shard_map.91) | data formatting | bytes 786432
where the time goes:
time: 49.9 us; the launch traced here: 49.7 us
  Pallas kernels  47.9 us (96%)
  local copies, waits for them, and re-layouts  1.77 us (4%)
    pallas_call x1, Pallas kernels, paired_body(): pl.pallas_call(functools.partial(layer_kernel, chunks), out_shape=jax.Sha...  47.9 us
    unnamed x1, local copies, waits for them, and re-layouts  1.77 us

commit v1 on v0

--- a/solution.py
+++ b/solution.py
@@ -84,16 +84,22 @@
 
 def layer_kernel(
     chunks,
+    group_hbm,
+    choice_hbm,
+    group_weight_hbm,
+    expert_weight_hbm,
+    gain_hbm,
+    tok_hbm,
+    gate_hbm,
+    up_hbm,
+    down_hbm,
+    out_ref,
     group_ref,
     choice_ref,
     group_weight_ref,
     expert_weight_ref,
     gain_ref,
     tok_ref,
-    gate_hbm,
-    up_hbm,
-    down_hbm,
-    out_ref,
     w_gate,
     w_up,
     w_down,
@@ -143,14 +149,21 @@
     model_width = 4 * width
     hidden_width = hid.shape[3]
 
+    pairs = (
+        (gate_hbm, w_gate),
+        (up_hbm, w_up),
+        (down_hbm, w_down),
+        (tok_hbm, tok_ref),
+        (group_hbm, group_ref),
+        (choice_hbm, choice_ref),
+        (group_weight_hbm, group_weight_ref),
+        (expert_weight_hbm, expert_weight_ref),
+        (gain_hbm, gain_ref),
+    )
     loads = [
         pltpu.make_async_copy(source, target, wsem.at[i])
-        for i, (source, target) in enumerate(
-            ((gate_hbm, w_gate), (up_hbm, w_up), (down_hbm, w_down))
-        )
+        for i, (source, target) in enumerate(pairs)
     ]
-    for load in loads:
-        load.start()
 
     barrier = pltpu.get_barrier_semaphore()
 
@@ -165,6 +178,9 @@
     @pl.when(is_inner)
     def _():
         greet(ep=cross_outer)
+
+    for i in (4, 3, 5, 6, 7, 8, 0, 1, 2):
+        loads[i].start()
 
     def remote(source, target, send, recv, **where):
         return pltpu.make_async_remote_copy(
@@ -186,6 +202,7 @@
     def column(row):
         return jnp.sum(jnp.where(eye, row, 0.0), 1, keepdims=True)
 
+    loads[4].wait()
     own_row = jnp.where(group_ref[...].reshape(1, -1) == group, 1.0, 0.0)
     own_rows = jnp.broadcast_to(own_row, (8, count)).astype(jnp.bfloat16)
     earlier = jnp.where(line < lane, 1.0, 0.0).astype(jnp.bfloat16)
@@ -207,6 +224,7 @@
     def keep_other(c, value):
         other[c] = value
 
+    loads[3].wait()
     sort_half(0, keep_own)
 
     pl.semaphore_wait(barrier, 4 + inner)
@@ -337,6 +355,8 @@
     for c in range(chunks):
         other_send(c).start()
     stage_a(1)
+    for i in (5, 6, 7, 8):
+        loads[i].wait()
     first, second = expert_weight_ref[0:1, :], expert_weight_ref[1:2, :]
     first_even = choice_ref[0:1, :] == 0
     scale = group_weight_ref[...].reshape(1, -1)
@@ -433,13 +453,19 @@
     bf16 = jnp.bfloat16
     dma = pltpu.SemaphoreType.DMA
     vmem = pl.BlockSpec(memory_space=pltpu.VMEM)
-    anywhere = pl.BlockSpec(memory_space=pl.ANY)
+    hbm = pl.BlockSpec(memory_space=pltpu.HBM)
     return pl.pallas_call(
         functools.partial(layer_kernel, chunks),
         out_shape=jax.ShapeDtypeStruct((count, width), bf16),
-        in_specs=[vmem] * 6 + [anywhere] * 3,
+        in_specs=[hbm] * 9,
         out_specs=vmem,
         scratch_shapes=[
+            pltpu.VMEM((count,), jnp.int32),
+            pltpu.VMEM((2, count), jnp.int32),
+            pltpu.VMEM((count,), jnp.float32),
+            pltpu.VMEM((2, count), jnp.float32),
+            pltpu.VMEM((1, norm_gain.shape[0]), jnp.float32),
+            pltpu.VMEM((count, width), bf16),
             pltpu.VMEM((depth, hidden_width), bf16),
             pltpu.VMEM((depth, hidden_width), bf16),
             pltpu.VMEM(w_down.shape[1:], bf16),
@@ -454,7 +480,7 @@
             pltpu.VMEM((8, count), jnp.float32),
             pltpu.VMEM((2, 8, count), jnp.float32),
             pltpu.VMEM((size, depth), bf16),
-            dma((3,)),
+            dma((9,)),
             dma((2 * chunks,)),
             dma((items,)),
             dma((2 * chunks,)),
@@ -470,9 +496,10 @@
             dma((2,)),
         ],
         compiler_params=pltpu.CompilerParams(
-            collective_id=0, has_side_effects=True, vmem_limit_bytes=56 * 1024 * 1024
+            collective_id=0, has_side_effects=True, vmem_limit_bytes=24 * 1024 * 1024
         ),
     )(
+        *[pltpu.with_memory_space_constraint(x, pltpu.HBM) for x in (
         group_choice,
         expert_choice.T,
         group_weight,
@@ -482,7 +509,7 @@
         w_gate[0],
         w_up[0],
         w_down[0],
-    )
+    )])
 
 def pick_body(mesh, *arrays):
     experts = arrays[6].shape[0]

time: 49.9 us -> 47.1 us (0.944)
  Pallas kernels: 47.9 us -> 46.1 us
  local copies, waits for them, and re-layouts: 1.77 us -> 0.75 us
    pallas_call x1, Pallas kernels: 47.9 us -> 46.1 us  [paired_body(): pl.pallas_call(functools.partial(layer_kernel, chunks), out_shape=jax.Sha...]
    unnamed x1, local copies, waits for them, and re-layouts: 1.77 us -> 0.75 us
where the time goes in v1:
time: 47.1 us; the launch traced here: 46.9 us
  Pallas kernels  46.1 us (98%)
  local copies, waits for them, and re-layouts  0.75 us (2%)
    pallas_call x1, Pallas kernels, paired_body(): pl.pallas_call(functools.partial(layer_kernel, chunks), out_shape=jax.Sha...  46.1 us

profile of v1, /device:TPU:0, one launch (start us, length us, event | category | flops | bytes accessed | tf_op | source)
XLA Modules:
  0.0 46.9 jit_solution(2925489085695258924)
XLA Ops:
  0.0 46.1 %shard_map.91 = bf16[384,512]{1,0:T(8,128)(2,1)S(1)} custom-call(s32[384]{0:T(512)} %group_hbm.1, s32[2,384]{1,0:T(2,128)} %bitcast.10, f32[384]{0:T(512)} %group_weight_hbm.1, f32[2,384]{1,0:T(2,128)} %bitcast.11, f32[1,2048]{1,0:T(1,128)} %bitcast.9, bf16[384,512]{1,0:T(8,128)(2,1)} %tok_hbm.1, bf16[2048,256]{1,0:T(8,128)(2,1)} %bitcast.6, ...), custom_call_target="tpu_custom_call" | custom-call | tf_op jit(solution)/shard_map/pallas_call | solution.py:457
  46.2 0.7 %copy.11 = bf16[384,512]{1,0:T(8,128)(2,1)} copy(bf16[384,512]{1,0:T(8,128)(2,1)S(1)} %shard_map.91) | data formatting | bytes 786432

commit v2 on v1

v2 whole, which is shorter than its diff:
```python
import functools

import jax
import jax.numpy as jnp
from jax import lax
from jax.experimental import pallas as pl
from jax.experimental.pallas import tpu as pltpu
from jax.sharding import PartitionSpec as P

MESH = pl.DeviceIdType.MESH


def finish_rows(gate_sum, up_sum, w_down):
    hidden = (jax.nn.silu(gate_sum) * up_sum).astype(jnp.bfloat16)
    whole_hidden = lax.all_gather(hidden, "tp", axis=3, tiled=True)
    summed = jnp.einsum("sxcf,xfd->sxcd", whole_hidden, w_down, preferred_element_type=jnp.float32)
    return summed.astype(jnp.bfloat16)


def body(
    tokens,
    group_choice,
    expert_choice,
    group_weight,
    expert_weight,
    norm_gain,
    w_gate,
    w_up,
    w_down,
):
    tok_rows = tokens.shape[0]
    ep_count = lax.axis_size("ep")
    exp_local = w_gate.shape[0]
    experts_all = ep_count * exp_local
    group_size = min(8, experts_all // 2)
    group_count = experts_all // group_size
    mean_load = 2 * tok_rows // experts_all
    capacity = mean_load + min(mean_load // 2, tok_rows // group_count - mean_load)
    model_width = norm_gain.shape[0]
    expert_ids = group_choice[:, None] * group_size + expert_choice
    mixing = group_weight[:, None] * expert_weight / jnp.sum(expert_weight, -1, keepdims=True)
    flat_ids = expert_ids.reshape(-1)
    marks = (flat_ids[:, None] == jnp.arange(experts_all, dtype=jnp.int32)[None, :]).astype(
        jnp.int32
    )
    earlier = jnp.cumsum(marks, 0) - marks
    seat_index = jnp.sum(earlier * marks, 1)
    targets = (flat_ids * capacity + seat_index).reshape(tok_rows, 2)
    places = jnp.arange(experts_all * capacity, dtype=jnp.int32)
    dispatch = (
        (places[:, None] == targets[None, :, 0]) | (places[:, None] == targets[None, :, 1])
    ).astype(jnp.bfloat16)
    values = tokens.astype(jnp.float32)
    own_squares = jnp.sum(values * values, -1)
    all_squares = lax.psum(own_squares, "tp")
    inv_rms = lax.rsqrt(all_squares / model_width + 1e-06)
    piece_width = tokens.shape[1]
    gain_piece = lax.dynamic_slice_in_dim(
        norm_gain, lax.axis_index("tp") * piece_width, piece_width, 0
    )
    normed = (values * inv_rms[:, None] * gain_piece[None, :]).astype(jnp.bfloat16)
    buffer = jnp.dot(dispatch, normed, preferred_element_type=jnp.float32).astype(jnp.bfloat16)
    buffer = buffer.reshape(ep_count, exp_local, capacity, piece_width)
    piece = lax.all_gather(
        lax.all_to_all(buffer, "ep", split_axis=0, concat_axis=0, tiled=True),
        "tp",
        axis=3,
        tiled=True,
    )
    gate_next = jnp.einsum("sxcd,xdf->sxcf", piece, w_gate, preferred_element_type=jnp.float32)
    up_next = jnp.einsum("sxcd,xdf->sxcf", piece, w_up, preferred_element_type=jnp.float32)
    results = finish_rows(gate_next, up_next, w_down)
    returned = lax.all_to_all(results, "ep", split_axis=0, concat_axis=0, tiled=True)
    returned = returned.reshape(experts_all * capacity, returned.shape[3])
    combined = jnp.zeros((tok_rows, returned.shape[1]), jnp.float32)
    for choice_index in range(2):
        picker = (targets[:, choice_index : choice_index + 1] == places[None, :]).astype(
            jnp.bfloat16
        )
        picked = jnp.dot(picker, returned, preferred_element_type=jnp.float32)
        combined = combined + mixing[:, choice_index : choice_index + 1] * picked
    return combined.astype(jnp.bfloat16)


def layer_kernel(
    chunks,
    fine,
    group_hbm,
    choice_hbm,
    group_weight_hbm,
    expert_weight_hbm,
    gain_hbm,
    tok_hbm,
    gate_hbm,
    up_hbm,
    down_hbm,
    out_ref,
    group_ref,
    choice_ref,
    group_weight_ref,
    expert_weight_ref,
    gain_ref,
    tok_ref,
    seat_ref,
    w_gate,
    w_up,
    w_down,
    rows,
    other,
    hid,
    outs,
    back,
    home,
    place,
    comb,
    mix_rows,
    mix_far,
    norm,
    wsem,
    z_send,
    z_recv,
    x_send,
    x_far,
    x_near,
    h_send,
    h_far,
    h_near,
    r_send,
    r_recv,
    c_send,
    c_recv,
    m_send,
    m_recv,
):
    z = lax.axis_index("ep")
    t = lax.axis_index("tp")
    group = z // 2
    parity = z % 2
    inner = (parity + group) % 2
    partner = z + 1 - 2 * parity
    cross = 2 - group
    cross_outer = 3 * (1 - group)
    near = t + 1 - 2 * (t % 2)
    far = (t + 2) % 4
    diag = (near + 2) % 4
    size, width = rows.shape[2:]
    half = size * fine
    each = fine // chunks
    count = 2 * half
    items = 4 * fine
    model_width = 4 * width
    hidden_width = hid.shape[3]

    pairs = (
        (gate_hbm, w_gate),
        (up_hbm, w_up),
        (down_hbm, w_down),
        (tok_hbm, tok_ref),
        (group_hbm, group_ref),
        (choice_hbm, choice_ref),
        (group_weight_hbm, group_weight_ref),
        (expert_weight_hbm, expert_weight_ref),
        (gain_hbm, gain_ref),
    )
    loads = [
        pltpu.make_async_copy(source, target, wsem.at[i])
        for i, (source, target) in enumerate(pairs)
    ]

    barrier = pltpu.get_barrier_semaphore()

    def greet(**where):
        pl.semaphore_signal(barrier, inc=1, device_id=where, device_id_type=MESH)

    greet(tp=near)
    greet(tp=far)
    greet(ep=partner)

    @pl.when(inner == 1)
    def _():
        greet(ep=cross)
        greet(ep=cross_outer)

    for i in (4, 3, 5, 6, 7, 8, 0, 1, 2):
        loads[i].start()

    def remote(source, target, send, recv, **where):
        return pltpu.make_async_remote_copy(
            src_ref=source,
            dst_ref=target,
            send_sem=send,
            recv_sem=recv,
            device_id=where,
            device_id_type=MESH,
        )

    def arrived(ref, sem):
        remote(ref, ref, sem, sem, tp=near).wait_recv()

    loads[4].wait()
    line = lax.broadcasted_iota(jnp.int32, (count, count), 0)
    lane = lax.broadcasted_iota(jnp.int32, (count, count), 1)
    own_row = jnp.where(group_ref[...].reshape(1, -1) == group, 1.0, 0.0)
    own_rows = jnp.broadcast_to(own_row, (8, count)).astype(jnp.bfloat16)
    earlier = jnp.where(line < lane, 1.0, 0.0).astype(jnp.bfloat16)
    before = jnp.dot(own_rows, earlier, preferred_element_type=jnp.float32)[0:1, :]
    at = lax.broadcasted_iota(jnp.int32, (1, count), 1).astype(jnp.float32)
    seat_row = jnp.where(own_row > 0.5, before, half + at - before)
    seat_ref[...] = seat_row

    def sort_half(start, target):
        want = lax.broadcasted_iota(jnp.int32, (half, count), 0) + start
        seat_ints = seat_ref[...].astype(jnp.int32)
        order = jnp.where(seat_ints == want, 1.0, 0.0).astype(jnp.bfloat16)
        part = jnp.dot(order, tok_ref[...], preferred_element_type=jnp.float32)
        for c in range(fine):
            target(c, part[c * size : (c + 1) * size].astype(jnp.bfloat16))

    def keep_own(c, value):
        rows[c, t] = value

    def keep_other(c, value):
        other[c] = value

    loads[3].wait()
    sort_half(0, keep_own)
    pl.semaphore_wait(barrier, 4)

    def drained(ref, sem):
        remote(ref, ref, sem, sem, tp=near).wait_send()

    def spread(buffer, k, send, over, beside):
        mine = buffer.at[k, t]
        remote(mine, mine, send, over, tp=far).start()
        remote(mine, mine, send, beside, tp=near).start()

    def pass_on(buffer, k, send, over, beside):
        theirs = buffer.at[k, far]
        arrived(theirs, over)
        remote(theirs, theirs, send, beside, tp=near).start()

    def normed(k):
        for i in range(each):
            item = k * each + i
            squares = jnp.zeros((size, 1), jnp.float32)
            for j in range(4):
                values = rows[item, j].astype(jnp.float32)
                squares = squares + jnp.sum(values * values, 1, keepdims=True)
            inv_rms = lax.rsqrt(squares / model_width + 1e-06)
            for j in range(4):
                cols = slice(j * width, (j + 1) * width)
                values = rows[item, j].astype(jnp.float32)
                norm[i * size : (i + 1) * size, cols] = (
                    values * inv_rms * gain_ref[0:1, cols]
                ).astype(jnp.bfloat16)

    def up_stage(k):
        gate = jnp.dot(norm[...], w_gate[...], preferred_element_type=jnp.float32)
        up = jnp.dot(norm[...], w_up[...], preferred_element_type=jnp.float32)
        hid[k, t] = (gate / (1.0 + jnp.exp(-gate)) * up).astype(jnp.bfloat16)

    def down_stage(k):
        total = jnp.zeros((size * each, width), jnp.float32)
        for j in range(4):
            part = w_down[j * hidden_width : (j + 1) * hidden_width, :]
            total = total + jnp.dot(hid[k, j], part, preferred_element_type=jnp.float32)
        for i in range(each):
            outs[k * each + i] = total[i * size : (i + 1) * size].astype(jnp.bfloat16)

    def mix_tables():
        first, second = expert_weight_ref[0:1, :], expert_weight_ref[1:2, :]
        first_even = choice_ref[0:1, :] == 0
        scale = group_weight_ref[...].reshape(1, -1)
        both = first + second
        even_row = scale * jnp.where(first_even, first, second) / both
        odd_row = scale * jnp.where(first_even, second, first) / both
        down = lax.broadcasted_iota(jnp.int32, (count, count), 0)
        over = lax.broadcasted_iota(jnp.int32, (count, count), 1)
        eye = down == over

        def column(row):
            return jnp.sum(jnp.where(eye, row, 0.0), 1, keepdims=True)

        seat_int = column(seat_ref[...]).astype(jnp.int32)
        taken = seat_int == over
        mix_rows[0:1, :] = jnp.sum(jnp.where(taken, column(even_row), 0.0), 0, keepdims=True)
        mix_rows[1:2, :] = jnp.sum(jnp.where(taken, column(odd_row), 0.0), 0, keepdims=True)
        wide = lax.broadcasted_iota(jnp.int32, (count, size), 1)
        for c in range(2 * fine):
            place[c] = jnp.where(seat_int == wide + c * size, 1.0, 0.0).astype(jnp.bfloat16)

    def joined(k, mixes, start, odd_first):
        start = start + (k % fine) * size
        low = lax.broadcasted_iota(jnp.int32, (size, count), 0) + start
        pick = low == lax.broadcasted_iota(jnp.int32, (size, count), 1)
        even = jnp.sum(jnp.where(pick, mixes[0:1, :], 0.0), 1, keepdims=True)
        odd = jnp.sum(jnp.where(pick, mixes[1:2, :], 0.0), 1, keepdims=True)
        mine, theirs = (odd, even) if odd_first else (even, odd)
        summed = mine * outs[k].astype(jnp.float32) + theirs * back[k].astype(jnp.float32)
        return summed.astype(jnp.bfloat16)

    def run(role):
        its_group, its_parity = role // 2, role % 2
        is_inner = (its_parity + its_group) % 2 == 1
        its_partner = role + 1 - 2 * its_parity
        its_cross = 2 - its_group
        its_cross_outer = 3 * (1 - its_group)
        slot = 2 if is_inner else 3
        waited = set()
        sums = [jnp.zeros((count, width), jnp.float32)]

        def once(name, wait):
            if name not in waited:
                waited.add(name)
                wait()

        def landed(k):
            once(("z", k), lambda: arrived(rows.at[k, t], z_recv.at[k - fine]))

        def send_row(source, k, place_at):
            sem = z_recv.at[k - fine]
            remote(source, rows.at[k, t], z_send, sem, ep=place_at).start()

        def send_back(k):
            there = k - fine if k < 2 * fine else k
            sem = r_recv.at[k - fine]
            remote(outs.at[k], back.at[there], r_send, sem, ep=its_partner).start()

        def send_home(k):
            where = its_cross if k < 3 * fine else its_cross_outer
            sem = c_recv.at[k % fine]
            remote(comb.at[k - 2 * fine], home.at[k % fine], c_send, sem, ep=where).start()

        def returned(k):
            arrived(back.at[k], r_recv.at[k if k < fine else k - fine])

        def act(step, k):
            if step == OWN:
                send_row(rows.at[k, t], fine + k, its_partner)
            elif step == SORT:
                sort_half(half, keep_other)
            elif step == OTHER:
                send_row(other.at[k], slot * fine + k, its_cross)
            elif step == MIX:
                for i in (5, 6, 7):
                    loads[i].wait()
                mix_tables()
                far_mix = mix_far.at[slot - 2]
                remote(mix_rows, far_mix, m_send, m_recv.at[slot - 2], ep=its_cross).start()
            elif step == ROW:
                if k >= fine:
                    landed(k)
                spread(rows, k, x_send, x_far.at[k], x_near.at[k // each])
            elif step == ROW_PASS:
                pass_on(rows, k, x_send, x_far.at[k], x_near.at[k // each])
            elif step == RELAY:
                landed(k)
                send_row(rows.at[k, t], k, its_partner)
            elif step == UP:
                arrived(rows.at[pl.ds(k * each, each), pl.ds(0, 2)], x_near.at[k])
                for i in (8, 0, 1):
                    once(("load", i), loads[i].wait)
                normed(k)
                up_stage(k)
            elif step == HID:
                spread(hid, k, h_send, h_far.at[k], h_near.at[k])
            elif step == HID_PASS:
                pass_on(hid, k, h_send, h_far.at[k], h_near.at[k])
            elif step == DOWN:
                arrived(hid.at[k, pl.ds(0, 2)], h_near.at[k])
                once(("load", 2), loads[2].wait)
                down_stage(k)
                if chunks <= k < 2 * chunks or (k >= 2 * chunks and not is_inner):
                    for i in range(each):
                        send_back(k * each + i)
            elif step == JOIN:
                i = k // fine - 2
                once(("mix", i), lambda: arrived(mix_far.at[i], m_recv.at[i]))
                returned(k)
                comb[k - 2 * fine] = joined(k, mix_far[i], half, its_parity)
                send_home(k)
            elif step == OWN_DONE:
                returned(k)
                done = joined(k, mix_rows[...], 0, its_parity)
                sums[0] += jnp.dot(place[k], done, preferred_element_type=jnp.float32)
            elif step == HOME_DONE:
                arrived(home.at[k], c_recv.at[k])
                done = home[k]
                sums[0] += jnp.dot(place[fine + k], done, preferred_element_type=jnp.float32)

        for step, k in PROGRAMS[role]:
            act(step, k)
        out_ref[...] = sums[0].astype(jnp.bfloat16)

        drained(rows.at[:, pl.ds(0, 3)], x_send)
        drained(hid.at[:, pl.ds(0, 3)], h_send)
        drained(mix_rows, m_send)
        if is_inner:
            drained(rows.at[pl.ds(0, fine)], z_send)
            drained(outs.at[pl.ds(0, fine)], r_send)
            drained(comb, c_send)
        else:
            drained(rows.at[pl.ds(0, fine), pl.ds(0, 2)], z_send)
            drained(outs.at[pl.ds(0, 3 * fine)], r_send)

    for role in range(len(PROGRAMS)):
        pl.when(z == role)(functools.partial(run, role))


CHUNKS = 3
FINE = 3
(
    OWN,
    SORT,
    OTHER,
    MIX,
    ROW,
    ROW_PASS,
    RELAY,
    UP,
    HID,
    HID_PASS,
    DOWN,
    JOIN,
    OWN_DONE,
    HOME_DONE,
) = range(14)
PROGRAMS = (
    (
        (ROW, 2),
        (OWN, 2),
        (ROW, 1),
        (SORT, 0),
        (OWN, 0),
        (ROW, 0),
        (OTHER, 1),
        (OTHER, 2),
        (ROW, 4),
        (ROW, 3),
        (OTHER, 0),
        (ROW, 7),
        (OWN, 1),
        (ROW_PASS, 4),
        (ROW, 5),
        (MIX, 0),
        (ROW, 10),
        (ROW, 8),
        (ROW_PASS, 3),
        (ROW_PASS, 1),
        (ROW_PASS, 7),
        (UP, 7),
        (HID, 7),
        (ROW, 11),
        (ROW_PASS, 0),
        (UP, 4),
        (ROW_PASS, 5),
        (ROW_PASS, 10),
        (UP, 1),
        (ROW_PASS, 8),
        (ROW, 6),
        (ROW_PASS, 2),
        (HID_PASS, 7),
        (UP, 8),
        (HID, 8),
        (UP, 10),
        (ROW_PASS, 11),
        (HID, 10),
        (DOWN, 7),
        (ROW, 9),
        (UP, 2),
        (UP, 11),
        (HID, 11),
        (HID, 4),
        (ROW_PASS, 6),
        (HID_PASS, 8),
        (UP, 3),
        (HID, 1),
        (DOWN, 8),
        (HID_PASS, 10),
        (UP, 0),
        (UP, 6),
        (HID, 6),
        (DOWN, 10),
        (HID_PASS, 11),
        (ROW_PASS, 9),
        (HID, 0),
        (UP, 5),
        (HID, 3),
        (DOWN, 11),
        (HID_PASS, 4),
        (UP, 9),
        (HID, 9),
        (HID_PASS, 1),
        (HID_PASS, 6),
        (DOWN, 4),
        (HID, 2),
        (DOWN, 1),
        (HID_PASS, 0),
        (HID, 5),
        (DOWN, 6),
        (HID_PASS, 3),
        (HID_PASS, 9),
        (DOWN, 0),
        (DOWN, 9),
        (HOME_DONE, 1),
        (HID_PASS, 2),
        (HID_PASS, 5),
        (DOWN, 3),
        (HOME_DONE, 2),
        (DOWN, 2),
        (DOWN, 5),
        (OWN_DONE, 0),
        (HOME_DONE, 0),
        (OWN_DONE, 2),
        (OWN_DONE, 1),
    ),
    (
        (ROW, 2),
        (OWN, 1),
        (OWN, 0),
        (OWN, 2),
        (SORT, 0),
        (ROW, 1),
        (ROW, 0),
        (OTHER, 1),
        (OTHER, 2),
        (ROW, 5),
        (RELAY, 7),
        (RELAY, 10),
        (ROW, 10),
        (ROW, 3),
        (ROW_PASS, 5),
        (RELAY, 8),
        (ROW, 8),
        (ROW_PASS, 2),
        (UP, 5),
        (OTHER, 0),
        (ROW_PASS, 1),
        (HID, 5),
        (ROW, 11),
        (RELAY, 11),
        (ROW, 7),
        (ROW_PASS, 3),
        (RELAY, 6),
        (ROW, 6),
        (ROW_PASS, 8),
        (HID_PASS, 5),
        (ROW_PASS, 0),
        (UP, 3),
        (RELAY, 9),
        (DOWN, 5),
        (HID, 3),
        (UP, 2),
        (ROW_PASS, 10),
        (UP, 8),
        (ROW_PASS, 7),
        (ROW, 4),
        (UP, 1),
        (ROW, 9),
        (UP, 10),
        (ROW_PASS, 6),
        (UP, 7),
        (HID_PASS, 3),
        (HID, 7),
        (ROW_PASS, 11),
        (HID, 2),
        (HID, 8),
        (HID, 10),
        (UP, 0),
        (DOWN, 3),
        (MIX, 0),
        (ROW_PASS, 4),
        (UP, 6),
        (ROW_PASS, 9),
        (UP, 11),
        (HID, 1),
        (HID, 6),
        (HID, 11),
        (HID_PASS, 7),
        (UP, 4),
        (HID_PASS, 2),
        (HID, 0),
        (DOWN, 7),
        (JOIN, 7),
        (HID_PASS, 8),
        (HID, 4),
        (DOWN, 2),
        (HID_PASS, 10),
        (DOWN, 8),
        (JOIN, 8),
        (HID_PASS, 1),
        (DOWN, 10),
        (UP, 9),
        (HID, 9),
        (HID_PASS, 11),
        (JOIN, 10),
        (DOWN, 1),
        (HID_PASS, 4),
        (HID_PASS, 6),
        (HID_PASS, 0),
        (DOWN, 11),
        (JOIN, 11),
        (DOWN, 0),
        (DOWN, 6),
        (DOWN, 4),
        (HID_PASS, 9),
        (JOIN, 6),
        (DOWN, 9),
        (OWN_DONE, 1),
        (JOIN, 9),
        (HOME_DONE, 1),
        (HOME_DONE, 2),
        (OWN_DONE, 0),
        (OWN_DONE, 2),
        (HOME_DONE, 0),
    ),
    (
        (ROW, 2),
        (ROW, 1),
        (OWN, 2),
        (SORT, 0),
        (OWN, 0),
        (OTHER, 1),
        (RELAY, 7),
        (OTHER, 2),
        (ROW, 7),
        (OWN, 1),
        (ROW, 3),
        (ROW, 0),
        (ROW_PASS, 2),
        (ROW_PASS, 1),
        (RELAY, 10),
        (RELAY, 8),
        (OTHER, 0),
        (ROW, 10),
        (RELAY, 11),
        (ROW_PASS, 7),
        (ROW, 11),
        (UP, 7),
        (HID, 7),
        (ROW, 8),
        (RELAY, 9),
        (ROW, 4),
        (ROW_PASS, 0),
        (UP, 2),
        (HID_PASS, 7),
        (RELAY, 6),
        (ROW_PASS, 10),
        (ROW, 5),
        (ROW_PASS, 3),
        (ROW_PASS, 11),
        (DOWN, 7),
        (ROW, 9),
        (UP, 3),
        (UP, 11),
        (HID, 11),
        (ROW_PASS, 4),
        (ROW_PASS, 8),
        (UP, 0),
        (HID, 3),
        (MIX, 0),
        (ROW_PASS, 5),
        (UP, 10),
        (UP, 1),
        (HID, 10),
        (ROW_PASS, 9),
        (UP, 5),
        (HID, 5),
        (HID_PASS, 11),
        (ROW, 6),
        (HID, 0),
        (HID_PASS, 3),
        (UP, 9),
        (DOWN, 11),
        (HID, 9),
        (HID_PASS, 10),
        (DOWN, 3),
        (UP, 4),
        (HID, 1),
        (HID_PASS, 5),
        (DOWN, 10),
        (UP, 8),
        (DOWN, 5),
        (HID, 8),
        (HID, 4),
        (ROW_PASS, 6),
        (HID, 2),
        (JOIN, 10),
        (HID_PASS, 9),
        (HID_PASS, 0),
        (UP, 6),
        (HID, 6),
        (HID_PASS, 1),
        (JOIN, 11),
        (HOME_DONE, 1),
        (DOWN, 0),
        (HID_PASS, 8),
        (DOWN, 9),
        (DOWN, 1),
        (HID_PASS, 4),
        (JOIN, 9),
        (HOME_DONE, 2),
        (HID_PASS, 2),
        (DOWN, 8),
        (HID_PASS, 6),
        (JOIN, 7),
        (DOWN, 4),
        (DOWN, 2),
        (DOWN, 6),
        (JOIN, 8),
        (JOIN, 6),
        (HOME_DONE, 0),
        (OWN_DONE, 1),
        (OWN_DONE, 0),
        (OWN_DONE, 2),
    ),
    (
        (ROW, 1),
        (OWN, 0),
        (ROW, 2),
        (SORT, 0),
        (ROW, 0),
        (MIX, 0),
        (OTHER, 1),
        (ROW, 5),
        (OTHER, 2),
        (ROW, 3),
        (ROW_PASS, 1),
        (ROW, 7),
        (ROW_PASS, 0),
        (OWN, 1),
        (OTHER, 0),
        (ROW_PASS, 2),
        (UP, 1),
        (OWN, 2),
        (ROW, 10),
        (ROW, 8),
        (UP, 0),
        (ROW_PASS, 3),
        (ROW_PASS, 7),
        (ROW, 11),
        (ROW, 4),
        (ROW_PASS, 5),
        (UP, 5),
        (ROW, 9),
        (ROW_PASS, 10),
        (UP, 7),
        (ROW_PASS, 8),
        (UP, 10),
        (HID, 10),
        (ROW_PASS, 11),
        (ROW_PASS, 4),
        (ROW, 6),
        (UP, 8),
        (UP, 3),
        (ROW_PASS, 9),
        (UP, 11),
        (HID, 11),
        (UP, 9),
        (HID, 9),
        (HID_PASS, 10),
        (HID, 7),
        (HID, 8),
        (DOWN, 10),
        (ROW_PASS, 6),
        (HID, 0),
        (HID, 1),
        (HID, 5),
        (HID_PASS, 11),
        (UP, 4),
        (HID_PASS, 9),
        (DOWN, 11),
        (HID_PASS, 7),
        (UP, 6),
        (HID_PASS, 8),
        (HID, 4),
        (DOWN, 9),
        (UP, 2),
        (HID_PASS, 0),
        (HID, 6),
        (DOWN, 7),
        (DOWN, 8),
        (HID_PASS, 1),
        (HID, 3),
        (DOWN, 0),
        (HID, 2),
        (HID_PASS, 5),
        (DOWN, 1),
        (HID_PASS, 6),
        (HID_PASS, 4),
        (DOWN, 6),
        (HID_PASS, 3),
        (DOWN, 4),
        (HID_PASS, 2),
        (HOME_DONE, 1),
        (DOWN, 3),
        (DOWN, 5),
        (DOWN, 2),
        (HOME_DONE, 2),
        (OWN_DONE, 2),
        (OWN_DONE, 1),
        (OWN_DONE, 0),
        (HOME_DONE, 0),
    ),
)


def paired_body(
    tokens,
    group_choice,
    expert_choice,
    group_weight,
    expert_weight,
    norm_gain,
    w_gate,
    w_up,
    w_down,
):
    count, width = tokens.shape
    half = count // 2
    depth, hidden_width = w_gate.shape[1:]
    chunks, fine = CHUNKS, FINE
    size = half // fine
    items = 4 * fine
    bf16 = jnp.bfloat16
    dma = pltpu.SemaphoreType.DMA
    vmem = pl.BlockSpec(memory_space=pltpu.VMEM)
    hbm = pl.BlockSpec(memory_space=pltpu.HBM)
    return pl.pallas_call(
        functools.partial(layer_kernel, chunks, fine),
        out_shape=jax.ShapeDtypeStruct((count, width), bf16),
        in_specs=[hbm] * 9,
        out_specs=vmem,
        scratch_shapes=[
            pltpu.VMEM((count,), jnp.int32),
            pltpu.VMEM((2, count), jnp.int32),
            pltpu.VMEM((count,), jnp.float32),
            pltpu.VMEM((2, count), jnp.float32),
            pltpu.VMEM((1, norm_gain.shape[0]), jnp.float32),
            pltpu.VMEM((count, width), bf16),
            pltpu.VMEM((1, count), jnp.float32),
            pltpu.VMEM((depth, hidden_width), bf16),
            pltpu.VMEM((depth, hidden_width), bf16),
            pltpu.VMEM(w_down.shape[1:], bf16),
            pltpu.VMEM((items, 4, size, width), bf16),
            pltpu.VMEM((fine, size, width), bf16),
            pltpu.VMEM((4 * chunks, 4, half // chunks, hidden_width), bf16),
            pltpu.VMEM((items, size, width), bf16),
            pltpu.VMEM((items, size, width), bf16),
            pltpu.VMEM((fine, size, width), bf16),
            pltpu.VMEM((2 * fine, count, size), bf16),
            pltpu.VMEM((2 * fine, size, width), bf16),
            pltpu.VMEM((8, count), jnp.float32),
            pltpu.VMEM((2, 8, count), jnp.float32),
            pltpu.VMEM((half // chunks, depth), bf16),
            dma((9,)),
            dma,
            dma((3 * fine,)),
            dma,
            dma((items,)),
            dma((4 * chunks,)),
            dma,
            dma((4 * chunks,)),
            dma((4 * chunks,)),
            dma,
            dma((3 * fine,)),
            dma,
            dma((fine,)),
            dma,
            dma((2,)),
        ],
        compiler_params=pltpu.CompilerParams(
            collective_id=0, has_side_effects=True, vmem_limit_bytes=24 * 1024 * 1024
        ),
    )(
        *[pltpu.with_memory_space_constraint(x, pltpu.HBM) for x in (
        group_choice,
        expert_choice.T,
        group_weight,
        expert_weight.T,
        norm_gain.reshape(1, -1),
        tokens,
        w_gate[0],
        w_up[0],
        w_down[0],
    )])


def pick_body(mesh, *arrays):
    experts = arrays[6].shape[0]
    group_size = min(8, experts // 2)
    choices = arrays[2].shape[1]
    sizes = dict(mesh.shape)
    fits = group_size == choices and experts == 2 * group_size == sizes["ep"]
    fits = fits and sizes["tp"] == sizes["ep"] == len(PROGRAMS)
    fits = fits and arrays[0].shape[0] % (32 * FINE) == 0
    return paired_body if fits else body


def solution(mesh):
    in_specs = (
        P(("grp", "ep"), "tp"),
        P(("grp", "ep")),
        P(("grp", "ep"), None),
        P(("grp", "ep")),
        P(("grp", "ep"), None),
        P(),
        P("ep", None, "tp"),
        P("ep", None, "tp"),
        P("ep", None, "tp"),
    )
    out_specs = P(("grp", "ep"), "tp")

    def layer(*arrays):
        run = jax.shard_map(
            pick_body(mesh, *arrays),
            mesh=mesh,
            in_specs=in_specs,
            out_specs=out_specs,
            check_vma=False,
        )
        return run(*arrays)

    return layer
```

time: 47.1 us -> 41.4 us (0.88)
  the two profiles are of different devices: /device:TPU:0 before, /device:TPU:9 now
where the time goes in v2:
time: 41.4 us; the launch traced here: 41.3 us
  Pallas kernels  40.5 us (98%)
  local copies, waits for them, and re-layouts  0.75 us (2%)
    pallas_call x1, Pallas kernels, paired_body(): pl.pallas_call(functools.partial(layer_kernel, chunks, fine), out_shape=j...  40.5 us

profile of v2, /device:TPU:9, one launch (start us, length us, event | category | flops | bytes accessed | tf_op | source)
XLA Modules:
  0.0 41.3 jit_solution(18184054340595413723)
XLA Ops:
  0.0 40.5 %shard_map.91 = bf16[384,512]{1,0:T(8,128)(2,1)S(1)} custom-call(s32[384]{0:T(512)} %group_hbm.1, s32[2,384]{1,0:T(2,128)} %bitcast.10, f32[384]{0:T(512)} %group_weight_hbm.1, f32[2,384]{1,0:T(2,128)} %bitcast.11, f32[1,2048]{1,0:T(1,128)} %bitcast.9, bf16[384,512]{1,0:T(8,128)(2,1)} %tok_hbm.1, bf16[2048,256]{1,0:T(8,128)(2,1)} %bitcast.6, ...), custom_call_target="tpu_custom_call" | custom-call | tf_op jit(solution)/shard_map/pallas_call | solution.py:829
  40.5 0.7 %copy.11 = bf16[384,512]{1,0:T(8,128)(2,1)} copy(bf16[384,512]{1,0:T(8,128)(2,1)S(1)} %shard_map.91) | data formatting | bytes 786432

commit v3 on v2

--- a/solution.py
+++ b/solution.py
@@ -493,22 +493,22 @@
         (HID_PASS, 1),
         (HID_PASS, 6),
         (DOWN, 4),
-        (HID, 2),
+        (HID, 5),
         (DOWN, 1),
         (HID_PASS, 0),
-        (HID, 5),
+        (HID, 2),
         (DOWN, 6),
         (HID_PASS, 3),
         (HID_PASS, 9),
         (DOWN, 0),
         (DOWN, 9),
         (HOME_DONE, 1),
+        (HID_PASS, 5),
         (HID_PASS, 2),
-        (HID_PASS, 5),
         (DOWN, 3),
+        (DOWN, 5),
         (HOME_DONE, 2),
         (DOWN, 2),
-        (DOWN, 5),
         (OWN_DONE, 0),
         (HOME_DONE, 0),
         (OWN_DONE, 2),
@@ -599,10 +599,10 @@
         (HID_PASS, 6),
         (HID_PASS, 0),
         (DOWN, 11),
+        (DOWN, 4),
         (JOIN, 11),
         (DOWN, 0),
         (DOWN, 6),
-        (DOWN, 4),
         (HID_PASS, 9),
         (JOIN, 6),
         (DOWN, 9),
@@ -772,12 +772,12 @@
         (DOWN, 11),
         (HID_PASS, 7),
         (UP, 6),
+        (HID, 6),
         (HID_PASS, 8),
         (HID, 4),
         (DOWN, 9),
         (UP, 2),
         (HID_PASS, 0),
-        (HID, 6),
         (DOWN, 7),
         (DOWN, 8),
         (HID_PASS, 1),

time: 41.4 us -> 41.1 us (level)
  the two profiles are of different devices: /device:TPU:9 before, /device:TPU:0 now
where the time goes in v3:
time: 41.1 us; the launch traced here: 40.5 us
  Pallas kernels  39.8 us (97%)
  local copies, waits for them, and re-layouts  0.75 us (2%)
    pallas_call x1, Pallas kernels, paired_body(): pl.pallas_call(functools.partial(layer_kernel, chunks, fine), out_shape=j...  39.8 us

profile of v3, /device:TPU:0, one launch (start us, length us, event | category | flops | bytes accessed | tf_op | source)
XLA Modules:
  0.0 40.5 jit_solution(3744936862648531996)
XLA Ops:
  0.0 39.8 %shard_map.91 = bf16[384,512]{1,0:T(8,128)(2,1)S(1)} custom-call(s32[384]{0:T(512)} %group_hbm.1, s32[2,384]{1,0:T(2,128)} %bitcast.10, f32[384]{0:T(512)} %group_weight_hbm.1, f32[2,384]{1,0:T(2,128)} %bitcast.11, f32[1,2048]{1,0:T(1,128)} %bitcast.9, bf16[384,512]{1,0:T(8,128)(2,1)} %tok_hbm.1, bf16[2048,256]{1,0:T(8,128)(2,1)} %bitcast.6, ...), custom_call_target="tpu_custom_call" | custom-call | tf_op jit(solution)/shard_map/pallas_call | solution.py:829
  39.8 0.7 %copy.11 = bf16[384,512]{1,0:T(8,128)(2,1)} copy(bf16[384,512]{1,0:T(8,128)(2,1)S(1)} %shard_map.91) | data formatting | bytes 786432
